TPU v7x, 512 devices: a whole 4x4x16 slice. The times are simulated.
512 devices in a mesh: fs: 16 (over y, x), tp: 32 (over z, core).
Axes of the slice: x: 4, y: 4, z: 16, core: 2. Of those that a mesh axis runs over, the one named last changes fastest.
Arguments:
- tokens: bfloat16 [16384, 2048], P(('fs', 'tp')), may hold values from -6 to 6
- norm_gain: float32 [2048], P('fs'), may hold values from 0.1 to 1.9
- gate_master: float32 [2048, 8192], P('fs', 'tp'), may hold values from -0.125 to 0.125
- up_master: float32 [2048, 8192], P('fs', 'tp'), may hold values from -0.125 to 0.125
- down_master: float32 [2048, 8192], P('fs', 'tp'), may hold values from -0.125 to 0.125
Outputs:
- mixed: bfloat16 [16384, 2048], P(('fs', 'tp'))
- gate_ready: bfloat16 [2048, 8192], P(None, 'tp')
- up_ready: bfloat16 [2048, 8192], P(None, 'tp')
- down_ready: bfloat16 [2048, 8192], P(None, 'tp')
All inputs are finite; a program needn't handle non-finite values.
Results may differ from a plain program's by a relative error of at most 0.0095.
Values may be sent and summed in bfloat16 or wider, within the bound.
A program may use at most 64 MiB of HBM per device.

v0:
```python
import jax
import jax.numpy as jnp
from jax import lax
from jax.sharding import Mesh
from jax.sharding import PartitionSpec as P

TP = ("tp_0", "tp_1")
FS_TP = ("fs", "tp_0", "tp_1")


def in_one_piece(arrays, axis, dim, along):
    both = jnp.concatenate(arrays, axis=along)
    whole, at, gathered = (lax.all_gather(both, axis, axis=dim, tiled=True), 0, [])
    for a in arrays:
        gathered.append(lax.slice_in_dim(whole, at, at + a.shape[along], axis=along))
        at += a.shape[along]
    return tuple(gathered)


def laid_out(parts, dim):
    dims = list(parts.shape[1:])
    dims[dim] *= parts.shape[0]
    return jnp.moveaxis(parts, 0, dim).reshape(dims)


def copy_for_each(array, axis):
    copies = jnp.broadcast_to(array, (lax.axis_size(axis), *array.shape))
    return lax.all_to_all(copies, axis, split_axis=0, concat_axis=0, tiled=True)


def collect(array, axis, dim):
    return laid_out(copy_for_each(array, axis), dim)


def own_block(parts, axes, sequence):
    inside = parts.shape[1:]
    parts = parts.reshape(*(lax.axis_size(a) for a in axes), *inside)
    parts = jnp.moveaxis(parts, sequence, range(len(axes))).reshape(-1, *inside)
    for k in sequence:
        parts = lax.psum_scatter(parts, axes[k], scatter_dimension=0, tiled=True)
    return parts[0]


def split_up(array, dim, length):
    dims = array.shape
    parts = array.reshape(*dims[:dim], length, dims[dim] // length, *dims[dim + 1 :])
    return jnp.moveaxis(parts, dim, 0)


def sum_by_axis(array, axes, sequence, dim):
    length = lax.axis_size(axes)
    return own_block(split_up(array, dim, length), axes, sequence)


def expand_rows(rows, gate_ready, up_ready):
    rows_wide = rows.astype(jnp.float32)
    row_scale = lax.rsqrt(jnp.mean(rows_wide * rows_wide, axis=1, keepdims=True) + 1e-06)
    gate_proj = row_scale * jnp.dot(rows, gate_ready, preferred_element_type=jnp.float32)
    up_proj = row_scale * jnp.dot(rows, up_ready, preferred_element_type=jnp.float32)
    return (jax.nn.silu(gate_proj) * up_proj).astype(jnp.bfloat16)


def body(tokens, norm_gain, gate_master, up_master, down_master):
    gate_local = (norm_gain[:, None] * gate_master).astype(jnp.bfloat16)
    up_local = (norm_gain[:, None] * up_master).astype(jnp.bfloat16)
    down_local = down_master.astype(jnp.bfloat16)
    gate_ready, up_ready = in_one_piece((gate_local, up_local), "fs", 0, 1)
    gathered = lax.all_gather(tokens, TP, axis=0, tiled=True)
    hidden = expand_rows(gathered, gate_ready, up_ready)
    down_ready = collect(down_local, "fs", 0)
    partial_value = lax.dot_general(
        hidden, down_ready, (((1,), (1,)), ((), ())), preferred_element_type=jnp.float32
    )
    summed = sum_by_axis(partial_value.astype(jnp.bfloat16), TP, (1, 0), 0).astype(jnp.float32)
    mixed = (tokens.astype(jnp.float32) + 0.5 * summed).astype(jnp.bfloat16)
    return (mixed, gate_ready, up_ready, down_ready)


def solution(mesh):
    split = Mesh(mesh.devices.reshape(mesh.shape["fs"], 16, 2), ("fs", "tp_0", "tp_1"))
    placed = (P(FS_TP, None), P("fs"), P("fs", TP), P("fs", TP), P("fs", TP))
    return jax.shard_map(
        body,
        mesh=split,
        in_specs=placed,
        out_specs=(P(FS_TP, None), P(None, TP), P(None, TP), P(None, TP)),
        check_vma=False,
    )
```

profile of v0, /device:TPU:6, one launch (start us, length us, event | category | flops | bytes accessed | tf_op | source)
XLA Modules:
  0.0 275.8 jit_solution(10192223352747149037)
XLA Ops:
  7.2 0.0 all-gather.5.cloned.1.call-start
  7.2 1.1 multiply_convert_fusion.1
  8.3 0.7 pad_maximum_fusion
  9.0 0.0 all-gather.5.cloned.1.call-update
  9.0 0.0 all-gather.3.cloned.1.call-start
  9.0 0.7 all-gather.3.cloned.1.call-update
  9.7 0.9 convert_element_type.33
  10.6 1.1 broadcast_in_dim.2
  11.7 9.3 %all-to-all-start = ((bf16[16,128,256]{2,1,0:T(8,128)(2,1)}), bf16[16,128,256]{2,1,0:T(8,128)(2,1)S(1)}, u32[]{:S(2)}, u32[]{:S(2)}) async-start(bf16[16,128,256]{2,1,0:T(8,128)(2,1)} %broadcast_in_dim.2), calls=%async_computation | async-start | bytes 2097152 | tf_op jit(solution)/shard_map/all_to_all | solution.py:28
  21.0 0.0 reduce-scatter.3.cloned.1.call-start
  21.0 54.8 %all-gather.5.cloned.1.call-done = bf16[2048,512]{1,0:T(8,128)(2,1)} async-done(((bf16[128,512]{1,0:T(8,128)(2,1)}), bf16[2048,512]{1,0:T(8,128)(2,1)}) %all-gather.5.cloned.1.call-update) | async-done | bytes 2097168 | tf_op jit(solution)/shard_map/all_gather | solution.py:13
  75.9 1.7 fusion.13
  77.6 0.0 copy-start.1
  77.6 0.0 copy-start.2
  77.6 73.6 %all-gather.3.cloned.1.call-done = bf16[1024,2048]{1,0:T(8,128)(2,1)} async-done(((bf16[32,2048]{1,0:T(8,128)(2,1)}), bf16[1024,2048]{1,0:T(8,128)(2,1)}) %all-gather.3.cloned.1.call-update) | async-done | bytes 4194320 | tf_op jit(solution)/shard_map/all_gather | solution.py:68
  151.2 0.0 copy-start
  151.2 3.2 %multiply_reduce_fusion = f32[1024]{0:T(1024)S(1)} fusion(bf16[1024,2048]{1,0:T(8,128)(2,1)} %all-gather.3.cloned.1.call-done), kind=kLoop, calls=%fused_computation | loop fusion | flops 6290432 | bytes 4198400 | tf_op jit(solution)/shard_map/reduce_sum | solution.py:57
  154.4 0.2 copy-done
  154.6 2.4 fusion.1
  157.0 0.0 copy-done.1
  157.0 0.0 all-to-all-done
  157.0 0.0 copy-done.2
  157.0 7.0 %convolution_convert_fusion = bf16[1024,2048]{1,0:T(8,128)(2,1)} fusion(bf16[2048,256]{1,0:T(8,128)(2,1)S(1)} %bitcast.26, bf16[2048,256]{1,0:T(8,128)(2,1)S(1)} %get-tuple-element.14, bf16[1024,2048]{1,0:T(8,128)(2,1)} %all-gather.3.cloned.1.call-done, f32[1024,256]{0,1:T(8,128)} %fusion.1, f32[1024]{0:T(1024)S(1)} %add_rsqrt_fusion), kind=kOutput, calls=%fused_computation.1 | convolution fusion | flops 2151415808 | bytes 11538432 | tf_op jit(solution)/shard_map/dot_general | solution.py:71
  164.0 4.7 %copy.9 = bf16[2,16,32,2048]{3,2,1,0:T(8,128)(2,1)} copy(bf16[2,16,32,2048]{3,2,0,1:T(8,128)(2,1)} %bitcast.25) | data formatting | bytes 8388608 | tf_op jit(solution)/shard_map/transpose | solution.py:38
  168.8 0.0 copy-start.3
  168.8 0.0 reduce-scatter.3.cloned.1.call-update
  168.8 0.0 reduce-scatter.5.cloned.1.call-start
  168.9 19.5 %reduce-scatter.3.cloned.1.call-done = bf16[16,32,2048]{2,1,0:T(8,128)(2,1)} async-done(((bf16[32,32,2048]{2,1,0:T(8,128)(2,1)}), bf16[16,32,2048]{2,1,0:T(8,128)(2,1)}) %reduce-scatter.3.cloned.1.call-update) | async-done | bytes 2097168 | tf_op jit(solution)/shard_map/reduce_scatter | solution.py:40
  188.4 0.0 reduce-scatter.5.cloned.1.call-update
  188.4 78.3 %reduce-scatter.5.cloned.1.call-done = bf16[1,32,2048]{2,1,0:T(8,128)(2,1)} async-done(((bf16[16,32,2048]{2,1,0:T(8,128)(2,1)}), bf16[1,32,2048]{2,1,0:T(8,128)(2,1)}) %reduce-scatter.5.cloned.1.call-update) | async-done | bytes 131088 | tf_op jit(solution)/shard_map/reduce_scatter | solution.py:40
  266.7 0.0 copy-done.3
  266.7 1.6 fusion.11
  268.3 1.0 copy.11
  (1 shorter events, 0.0 us)
Async XLA Ops:
  7.2 68.7 %all-gather.5.cloned.1.call-start = ((), (), s32[]{:S(2)}) async-start(), calls=%async_computation.4 | async-start | bytes 2228224 | tf_op jit(solution)/shard_map/all_gather | solution.py:13
  9.0 142.2 %all-gather.3.cloned.1.call-start = ((), (), s32[]{:S(2)}) async-start(), calls=%async_computation.3 | async-start | bytes 4325376 | tf_op jit(solution)/shard_map/all_gather | solution.py:68
  11.7 145.3 %all-to-all-start = ((bf16[16,128,256]{2,1,0:T(8,128)(2,1)}), bf16[16,128,256]{2,1,0:T(8,128)(2,1)S(1)}, u32[]{:S(2)}, u32[]{:S(2)}) async-start(bf16[16,128,256]{2,1,0:T(8,128)(2,1)} %broadcast_in_dim.2), calls=%async_computation | async-start | bytes 2097152 | tf_op jit(solution)/shard_map/all_to_all | solution.py:28
  21.0 167.4 %reduce-scatter.3.cloned.1.call-start = ((), (), s32[]{:S(2)}) async-start(), calls=%async_computation.5 | async-start | bytes 6291456 | tf_op jit(solution)/shard_map/reduce_scatter | solution.py:40
  77.6 79.4 %copy-start.1 = (bf16[2048,256]{1,0:T(8,128)(2,1)}, bf16[2048,256]{1,0:T(8,128)(2,1)S(1)}, u32[]{:S(2)}) copy-start(bf16[2048,256]{1,0:T(8,128)(2,1)S(1)} %get-tuple-element.13) | copy-start | bytes 3145732
  77.6 79.4 %copy-start.2 = (bf16[2048,256]{1,0:T(8,128)(2,1)}, bf16[2048,256]{1,0:T(8,128)(2,1)S(1)}, u32[]{:S(2)}) copy-start(bf16[2048,256]{1,0:T(8,128)(2,1)S(1)} %get-tuple-element.14) | copy-start | bytes 3145732
  151.2 3.4 %copy-start = (bf16[1024,2048]{1,0:T(8,128)(2,1)S(1)}, bf16[1024,2048]{1,0:T(8,128)(2,1)}, u32[]{:S(2)}) copy-start(bf16[1024,2048]{1,0:T(8,128)(2,1)} %all-gather.3.cloned.1.call-done) | copy-start | bytes 12582916
  168.8 97.9 %copy-start.3 = (bf16[32,2048]{1,0:T(8,128)(2,1)S(1)}, bf16[32,2048]{1,0:T(8,128)(2,1)}, u32[]{:S(2)}) copy-start(bf16[32,2048]{1,0:T(8,128)(2,1)} %param.5) | copy-start | bytes 393220
  168.8 97.9 %reduce-scatter.5.cloned.1.call-start = ((), (), s32[]{:S(2)}) async-start(), calls=%async_computation.6 | async-start | bytes 2228224 | tf_op jit(solution)/shard_map/reduce_scatter | solution.py:40
Sparse Core Ops, SparseCore 0:
  11.6 64.2 all-gather.4
  78.0 73.1 all-gather.2
  168.9 19.3 reduce-scatter.2
  191.0 75.5 reduce-scatter.4
where the time goes:
time: 276 us
  waiting for transfers between devices  227 us (82%)
  between operations  13.8 us (5%)
  starting transfers between devices  9.44 us (3%)
  matrix products  9.4 us (3%)
  local copies, waits for them, and re-layouts  8.68 us (3%)
  other arithmetic  7.48 us (3%)
    reduce_scatter x2, waiting for transfers between devices, own_block(): parts = lax.psum_scatter(parts, axes[k], scatter_dimension=0, tiled=True)  97.8 us
    all_gather x1, waiting for transfers between devices, body(): gathered = lax.all_gather(tokens, TP, axis=0, tiled=True)  73.6 us
    all_gather x1, waiting for transfers between devices, in_one_piece(): lax.all_gather(both, axis, axis=dim, tiled=True)  54.8 us
    all_to_all x1, starting transfers between devices, copy_for_each(): return lax.all_to_all(copies, axis, split_axis=0, concat_axis=0, tiled=True)  9.28 us
    dot_general x1, matrix products, body(): lax.dot_general(hidden, down_ready, (((1,), (1,)), ((), ())), preferred_e...  7.04 us
  transfers between devices with their start and end apart: 5, of which 4 were waited for; matrix products, arithmetic and copies ran while one was open for 3% of the time, Pallas kernels for 0%

commit v1 on v0

v1 whole, which is shorter than its diff:
```python
import jax
import jax.numpy as jnp
from jax import lax
from jax.experimental import pallas as pl
from jax.experimental.pallas import tpu as pltpu
from jax.sharding import Mesh
from jax.sharding import PartitionSpec as P

AXES = ("y", "x", "z", "c")
NZ = 16
NR = 4
HOPS = NZ // 2
NC = 8
CW = 256
ROWS = 32
D = 2048
W_DELAY = 8
MESH = pl.DeviceIdType.MESH


def kernel(tok, gain, gate_m, up_m, down_m, mixed, gate_o, up_o, down_o,
           T, W, M, G, H, PS, RV, SD, O,
           load_sem, tok_sem, ag_s, ag_r, rs_s, rs_r, xy_s, xy_r, dd_s, dd_r, out_sem):
    y, x, z, c = (lax.axis_index(a) for a in AXES)
    zto = ({"z": (z + 1) % NZ}, {"z": (z + NZ - 1) % NZ})
    f = 1 - 2 * c
    here = (x, y)
    names = ("x", "y")

    tok_loads = [pltpu.make_async_copy(tok.at[:, pl.ds(q * CW, CW)], T.at[z, q], tok_sem) for q in range(NC)]
    for copy in tok_loads:
        copy.start()
    gain_load = pltpu.make_async_copy(gain, G, load_sem.at[0])
    gain_load.start()
    m_loads = [pltpu.make_async_copy(src, M.at[j], load_sem.at[1 + j]) for j, src in enumerate((gate_m, up_m, down_m))]
    for copy in m_loads:
        copy.start()

    barrier = pltpu.get_barrier_semaphore()
    peers = [zto[0], zto[1], {"c": 1 - c}]
    for a in range(2):
        peers += [{names[a]: (here[a] + 1) % NR}, {names[a]: (here[a] + NR - 1) % NR}]
    for peer in peers:
        pl.semaphore_signal(barrier, inc=1, device_id=peer, device_id_type=MESH)

    own = y * NR + x
    gain_load.wait()
    g = jnp.broadcast_to(G[...], (128, 128)).T
    g = jnp.concatenate([g, g], axis=1)
    for j in range(3):
        m_loads[j].wait()
        value = M[j] * g if j < 2 else M[j]
        W[c, j, own] = value.astype(jnp.bfloat16).reshape(2, 64, 256)

    pltpu.make_async_copy(T.at[z], T.at[z], tok_sem).wait()
    pl.semaphore_wait(barrier, len(peers))

    def token_copy(way, step, q):
        block = (z + NZ - (step - 1)) % NZ if way == 0 else (z + step - 1) % NZ
        return pltpu.make_async_remote_copy(
            src_ref=T.at[block, q], dst_ref=T.at[block, q],
            send_sem=ag_s.at[way, 1 if step == HOPS else 0], recv_sem=ag_r.at[way, step - 1, q],
            device_id=zto[way], device_id_type=MESH)

    def token_wait(way, step, q):
        block = (z + NZ - step) % NZ if way == 0 else (z + step) % NZ
        pltpu.make_async_remote_copy(
            src_ref=T.at[block, q], dst_ref=T.at[block, q],
            send_sem=ag_s.at[way, 0], recv_sem=ag_r.at[way, step - 1, q],
            device_id=zto[way], device_id_type=MESH).wait_recv()

    def goes(way, q):
        return q < NC // 2 if way == 0 else q >= NC // 2

    def order(way, j):
        return j if way == 0 else (j + NC // 2) % NC

    for j in range(NC):
        for way in range(2):
            token_copy(way, 1, order(way, j)).start()

    def piece(h, r1, r2):
        a1 = here[h] + r1
        a2 = here[1 - h] + r2
        a1, a2 = (a1 + 2 * NR) % NR, (a2 + 2 * NR) % NR
        i = a2 * NR + a1 if h == 0 else a1 * NR + a2
        return W.at[c, :, i, h]

    off = (0, -f, f, 2)

    def weight_copy(h, ref, axis, sign, event):
        a = h if axis == 0 else 1 - h
        return pltpu.make_async_remote_copy(
            src_ref=ref, dst_ref=ref, send_sem=xy_s, recv_sem=xy_r.at[h * 15 + event],
            device_id={names[a]: (here[a] + sign * f + NR) % NR}, device_id_type=MESH)

    def sibling_copy(ref):
        return pltpu.make_async_remote_copy(
            src_ref=ref, dst_ref=ref, send_sem=dd_s, recv_sem=dd_r,
            device_id={"c": 1 - c}, device_id_type=MESH)

    for h in range(2):
        mine = piece(h, 0, 0)
        weight_copy(h, mine, 0, 1, 0).start()
        weight_copy(h, mine, 0, -1, 1).start()
    for h in range(2):
        mine = piece(h, 0, 0)
        weight_copy(h, mine, 1, 1, 3).start()
        weight_copy(h, mine, 1, -1, 7).start()
        sibling_copy(mine).start()

    def weight_event(h, event):
        if event < 3:
            r = event + 1
            ref = piece(h, off[r], 0)
        else:
            kind, r = divmod(event - 3, 4)
            ref = piece(h, off[r], (-f, f, 2)[kind])
        weight_copy(h, ref, 0, 1, event).wait_recv()
        if event == 0:
            weight_copy(h, ref, 0, 1, 2).start()
        if event < 3:
            weight_copy(h, ref, 1, 1, 3 + r).start()
            weight_copy(h, ref, 1, -1, 7 + r).start()
        elif event < 7:
            weight_copy(h, ref, 1, 1, 11 + r).start()
        sibling_copy(ref).start()

    weight_order = [(h, e) for e in (0, 1, 3, 7, 2, 4, 8, 5, 9, 11, 6, 10, 12, 13, 14) for h in range(2)]

    done = 0
    for step in range(1, HOPS + 1):
        for j in range(NC if step < HOPS else NC // 2):
            for way in range(2):
                q = order(way, j)
                token_wait(way, step, q)
                if step + 1 < HOPS or (step + 1 == HOPS and goes(way, q)):
                    token_copy(way, step + 1, q).start()
            due = ((step - 1) * NC + j - W_DELAY) * 5 // NC
            while done < min(due, 30):
                weight_event(*weight_order[done])
                done += 1
    while done < 30:
        weight_event(*weight_order[done])
        done += 1

    outs = [pltpu.make_async_copy(W.at[c, j], o, out_sem.at[j]) for j, o in enumerate((gate_o, up_o, down_o))]
    for copy in outs:
        copy.start()
    theirs = W.at[1 - c]
    pltpu.make_async_remote_copy(
        src_ref=theirs, dst_ref=theirs, send_sem=dd_s, recv_sem=dd_r,
        device_id={"c": 1 - c}, device_id_type=MESH).wait_recv()

    def expand(m, carry):
        parts = [T[pl.ds(m * 8, 8), q].reshape(256, CW) for q in range(NC)]
        total = jnp.zeros((256, 1), jnp.float32)
        for part in parts:
            wide = part.astype(jnp.float32)
            total = total + jnp.sum(wide * wide, axis=1, keepdims=True)
        scale = lax.rsqrt(total * (1.0 / D) + 1e-06)
        rows = jnp.concatenate(parts, axis=1)
        for k in range(2):
            gate = scale * jnp.dot(rows, W[k, 0].reshape(D, 256), preferred_element_type=jnp.float32)
            up = scale * jnp.dot(rows, W[k, 1].reshape(D, 256), preferred_element_type=jnp.float32)
            hid = gate / (1.0 + jnp.exp(-gate)) * up
            H[pl.ds(pl.multiple_of(m * 256, 256), 256), k * 256 : (k + 1) * 256] = hid.astype(jnp.bfloat16)
        return carry

    lax.fori_loop(0, 2, expand, 0)

    def dest(way, step):
        return (z + HOPS - step) % NZ if way == 0 else (z + HOPS + step) % NZ

    def sum_copy(way, step, q):
        return pltpu.make_async_remote_copy(
            src_ref=SD.at[way, step, q], dst_ref=RV.at[way, step, q],
            send_sem=rs_s.at[way, 1 if step == 0 else 0], recv_sem=rs_r.at[way, step, q],
            device_id=zto[way], device_id_type=MESH)

    for q in range(NC):
        value = None
        for k in range(2):
            part = lax.dot_general(H[:, k * 256 : (k + 1) * 256], W[k, 2, 2 * q : 2 * q + 2].reshape(256, 256),
                                   (((1,), (1,)), ((), ())), preferred_element_type=jnp.float32)
            value = part if value is None else value + part
        PS[:, q] = value.reshape(NZ, ROWS, CW)
        first = 0 if goes(0, q) else 1
        for way, step in ((first, 0), (1 - first, 1)):
            SD[way, step, q] = PS[dest(way, step), q].astype(jnp.bfloat16)
        for way, step in ((first, 0), (1 - first, 1)):
            sum_copy(way, step, q).start()

    for step in range(1, HOPS):
        for j in range(NC if step > 1 else NC // 2):
            for way in range(2):
                q = order(way, j) if step == 1 else order(1 - way, j)
                sum_copy(way, step - 1, q).wait_recv()
                SD[way, step, q] = (PS[dest(way, step), q] + RV[way, step - 1, q].astype(jnp.float32)).astype(jnp.bfloat16)
                sum_copy(way, step, q).start()

    last = []
    for q in range(NC):
        total = PS[z, q]
        for way in range(2):
            sum_copy(way, HOPS - 1, q).wait_recv()
            total = total + RV[way, HOPS - 1, q].astype(jnp.float32)
        O[:, q * CW : (q + 1) * CW] = (T[z, q].astype(jnp.float32) + 0.5 * total).astype(jnp.bfloat16)
    last = pltpu.make_async_copy(O, mixed, out_sem.at[3])
    last.start()

    def sent(ref, sem):
        pltpu.make_async_copy(ref, ref, sem).wait()

    for way in range(2):
        sent(T.at[pl.ds(0, HOPS - 1)], ag_s.at[way, 0])
        sent(T.at[0, pl.ds(0, NC // 2)], ag_s.at[way, 1])
        sent(T.at[pl.ds(0, HOPS - 1)], rs_s.at[way, 0])
        sent(T.at[0, pl.ds(0, NC // 2)], rs_s.at[way, 1])
    sent(W.at[0, :, pl.ds(0, 15)], xy_s)
    sent(W.at[0], dd_s)
    for copy in outs:
        copy.wait()
    last.wait()


def body(tokens, norm_gain, gate_master, up_master, down_master):
    ready = jax.ShapeDtypeStruct((16, 2, 64, 256), jnp.bfloat16)
    whole = pl.BlockSpec(memory_space=pl.ANY)
    dma = pltpu.SemaphoreType.DMA
    mixed, gate, up, down = pl.pallas_call(
        kernel,
        out_shape=(jax.ShapeDtypeStruct((ROWS, D), jnp.bfloat16), ready, ready, ready),
        in_specs=[whole] * 5,
        out_specs=(whole,) * 4,
        scratch_shapes=[
            pltpu.VMEM((NZ, NC, ROWS, CW), jnp.bfloat16),
            pltpu.VMEM((2, 3, 16, 2, 64, 256), jnp.bfloat16),
            pltpu.VMEM((3, 128, 256), jnp.float32),
            pltpu.VMEM((1, 128), jnp.float32),
            pltpu.VMEM((NZ * ROWS, 512), jnp.bfloat16),
            pltpu.VMEM((NZ, NC, ROWS, CW), jnp.float32),
            pltpu.VMEM((2, HOPS, NC, ROWS, CW), jnp.bfloat16),
            pltpu.VMEM((2, HOPS, NC, ROWS, CW), jnp.bfloat16),
            pltpu.VMEM((ROWS, D), jnp.bfloat16),
            dma((4,)),
            dma,
            dma((2, 2)),
            dma((2, HOPS, NC)),
            dma((2, 2)),
            dma((2, HOPS, NC)),
            dma,
            dma((30,)),
            dma,
            dma,
            dma((4,)),
        ],
        compiler_params=pltpu.CompilerParams(collective_id=0, has_side_effects=True, vmem_limit_bytes=50 * 2**20),
    )(tokens, norm_gain.reshape(1, 128), gate_master, up_master, down_master)
    return mixed, gate.reshape(D, 256), up.reshape(D, 256), down.reshape(D, 256)


def solution(mesh):
    split = Mesh(mesh.devices.reshape(NR, NR, NZ, 2), AXES)
    fs, tp = ("y", "x"), ("z", "c")
    return jax.shard_map(
        body,
        mesh=split,
        in_specs=(P(fs + tp, None), P(fs), P(fs, tp), P(fs, tp), P(fs, tp)),
        out_specs=(P(fs + tp, None), P(None, tp), P(None, tp), P(None, tp)),
        check_vma=False,
    )
```

time: 276 us -> 82.6 us (0.30)
  waiting for transfers between devices: 227 us -> 0 us
  Pallas kernels: 0 us -> 73.7 us
  between operations: 13.8 us -> 0.65 us
  starting transfers between devices: 9.44 us -> 0 us
  matrix products: 9.4 us -> 0 us
  other arithmetic: 7.48 us -> 0 us
    all_gather x2 -> x0, waiting for transfers between devices: 128 us -> none  [the longest x1 73.6 us: body(): gathered = lax.all_gather(tokens, TP, axis=0, tiled=True)]
    reduce_scatter x2 -> x0, waiting for transfers between devices: 97.8 us -> none  [own_block(): parts = lax.psum_scatter(parts, axes[k], scatter_dimension=0, tiled=True)]
    pallas_call x0 -> x1, Pallas kernels: none -> 73.7 us  [body(): pl.pallas_call(kernel, out_shape=(jax.ShapeDtypeStruct((ROWS, D), jnp.bfl...]
    dot_general x2 -> x0, matrix products: 9.4 us -> none  [the longest x1 7.04 us: body(): lax.dot_general(hidden, down_ready, (((1,), (1,)), ((), ())), preferred_e...]
    all_to_all x1 -> x0, starting transfers between devices: 9.28 us -> none  [copy_for_each(): return lax.all_to_all(copies, axis, split_axis=0, concat_axis=0, tiled=True)]
    unnamed x9 -> x14, local copies, waits for them, and re-layouts: 1.2 us -> 7.83 us
    transpose x1 -> x0, local copies, waits for them, and re-layouts: 4.73 us -> none  [own_block(): parts = jnp.moveaxis(parts, sequence, range(len(axes))).reshape(-1, *inside)]
    convert_element_type x3 -> x0, other arithmetic: 3.58 us -> none  [the longest x1 1.6 us: body(): mixed = (tokens.astype(jnp.float32) + 0.5 * summed).astype(jnp.bfloat16)]
  transfers between devices with their start and end apart: 5 -> 0, of which waited for: 4 -> 0; matrix products, arithmetic and copies ran while one was open for 3% -> 0% of each run, Pallas kernels for 0% -> 0%
where the time goes in v1:
time: 82.6 us; the launch traced here: 82.2 us
  Pallas kernels  73.7 us (89%)
  local copies, waits for them, and re-layouts  7.83 us (9%)
    pallas_call x1, Pallas kernels, body(): pl.pallas_call(kernel, out_shape=(jax.ShapeDtypeStruct((ROWS, D), jnp.bfl...  73.7 us
    unnamed x14, local copies, waits for them, and re-layouts  7.83 us

profile of v1, /device:TPU:6, one launch (start us, length us, event | category | flops | bytes accessed | tf_op | source)
XLA Modules:
  0.0 82.2 jit_solution(1391505372774384174)
XLA Ops:
  0.6 0.0 copy-start.4
  0.6 0.6 copy-done.4
  1.3 0.0 copy-start
  1.3 0.9 %copy-done = bf16[32,2048]{1,0:T(8,128)(2,1)S(1)} copy-done((bf16[32,2048]{1,0:T(8,128)(2,1)S(1)}, bf16[32,2048]{1,0:T(8,128)(2,1)}, u32[]{:S(2)}) %copy-start) | copy-done | bytes 131096
  2.2 0.0 copy-start.1
  2.2 0.9 %copy-done.1 = f32[128,256]{1,0:T(8,128)S(1)} copy-done((f32[128,256]{1,0:T(8,128)S(1)}, f32[128,256]{1,0:T(8,128)}, u32[]{:S(2)}) %copy-start.1) | copy-done | bytes 131096
  3.1 0.0 copy-start.2
  3.1 0.9 %copy-done.2 = f32[128,256]{1,0:T(8,128)S(1)} copy-done((f32[128,256]{1,0:T(8,128)S(1)}, f32[128,256]{1,0:T(8,128)}, u32[]{:S(2)}) %copy-start.2) | copy-done | bytes 131096
  4.0 0.0 copy-start.3
  4.0 0.9 %copy-done.3 = f32[128,256]{1,0:T(8,128)S(1)} copy-done((f32[128,256]{1,0:T(8,128)S(1)}, f32[128,256]{1,0:T(8,128)}, u32[]{:S(2)}) %copy-start.3) | copy-done | bytes 131096
  4.9 73.7 %shard_map.84 = (bf16[32,2048]{1,0:T(8,128)(2,1)S(1)}, bf16[16,2,64,256]{3,2,1,0:T(8,128)(2,1)S(1)}, bf16[16,2,64,256]{3,2,1,0:T(8,128)(2,1)S(1)}, bf16[16,2,64,256]{3,2,1,0:T(8,128)(2,1)S(1)}) custom-call(bf16[32,2048]{1,0:T(8,128)(2,1)S(1)} %copy-done, f32[1,128]{1,0:T(1,128)S(1)} %bitcast.7, f32[128,256]{1,0:T(8,128)S(1)} %copy-done.1, ...), custom_call_target="tpu_custom_call" | custom-call | tf_op jit(solution)/shard_map/pallas_call | solution.py:231
  78.6 0.7 copy.13
  79.3 1.0 %copy.14 = bf16[2048,256]{1,0:T(8,128)(2,1)} copy(bf16[2048,256]{1,0:T(8,128)(2,1)S(1)} %bitcast.6) | data formatting | bytes 2097152
  80.3 1.0 %copy.15 = bf16[2048,256]{1,0:T(8,128)(2,1)} copy(bf16[2048,256]{1,0:T(8,128)(2,1)S(1)} %bitcast.5) | data formatting | bytes 2097152
  81.2 1.0 %copy.16 = bf16[2048,256]{1,0:T(8,128)(2,1)} copy(bf16[2048,256]{1,0:T(8,128)(2,1)S(1)} %bitcast.4) | data formatting | bytes 2097152
Async XLA Ops:
  0.6 0.7 copy-start.4
  1.3 0.9 %copy-start = (bf16[32,2048]{1,0:T(8,128)(2,1)S(1)}, bf16[32,2048]{1,0:T(8,128)(2,1)}, u32[]{:S(2)}) copy-start(bf16[32,2048]{1,0:T(8,128)(2,1)} %tok.1) | copy-start | bytes 393220
  2.2 0.9 %copy-start.1 = (f32[128,256]{1,0:T(8,128)S(1)}, f32[128,256]{1,0:T(8,128)}, u32[]{:S(2)}) copy-start(f32[128,256]{1,0:T(8,128)} %gate_m.1) | copy-start | bytes 393220
  3.1 0.9 %copy-start.2 = (f32[128,256]{1,0:T(8,128)S(1)}, f32[128,256]{1,0:T(8,128)}, u32[]{:S(2)}) copy-start(f32[128,256]{1,0:T(8,128)} %up_m.1) | copy-start | bytes 393220
  4.0 0.9 %copy-start.3 = (f32[128,256]{1,0:T(8,128)S(1)}, f32[128,256]{1,0:T(8,128)}, u32[]{:S(2)}) copy-start(f32[128,256]{1,0:T(8,128)} %down_m.1) | copy-start | bytes 393220
